TPU v7x, 32 devices: a whole 2x2x4 slice. The times are simulated.
32 devices in a mesh: ep: 8 (over z, y), tp: 4 (over x, core).
Axes of the slice: x: 2, y: 2, z: 4, core: 2. Of those that a mesh axis runs over, the one named last changes fastest.
Arguments:
- resid: bfloat16 [256, 2048], P('ep'), may hold values from -6 to 6
- mix_gain: bfloat16 [2048], replicated, may hold values from 0.099609375 to 1.8984375
- proj_x: bfloat16 [2048, 512], P(None, 'tp'), may hold values from -0.125 to 0.125
- proj_z: bfloat16 [2048, 512], P(None, 'tp'), may hold values from -0.125 to 0.125
- proj_b: bfloat16 [2048, 512], P(None, 'tp'), may hold values from -0.125 to 0.125
- proj_c: bfloat16 [2048, 512], P(None, 'tp'), may hold values from -0.125 to 0.125
- proj_step: bfloat16 [2048, 8], replicated, may hold values from -0.125 to 0.125
- step_bias: float32 [8], P('tp'), may hold values from -5 to -1
- decay_rate: float32 [8], P('tp'), may hold values from 1 to 16
- conv_taps: bfloat16 [3, 4, 512], P(None, None, 'tp'), may hold values from -3 to 3
- conv_state: bfloat16 [256, 3, 3, 512], P('ep', None, None, 'tp'), may hold values from -6 to 6
- scan_state: float32 [256, 8, 64, 128], P('ep', 'tp'), may hold values from -2.5 to 2.5
- inner_gain: bfloat16 [512], P('tp'), may hold values from 0.099609375 to 1.8984375
- proj_out: bfloat16 [512, 2048], P('tp'), may hold values from -0.25 to 0.25
- post_gain: bfloat16 [2048], replicated, may hold values from 0.099609375 to 1.8984375
- ffn_gain: bfloat16 [2048], replicated, may hold values from 0.099609375 to 1.8984375
- group_router: bfloat16 [2048, 2], replicated, may hold values from -0.125 to 0.125
- expert_router: bfloat16 [2048, 8], replicated, may hold values from -0.125 to 0.125
- route_experts: int32 [256, 4], P('ep'), may hold values from 0 to 7, as said below
- expert_gate: bfloat16 [8, 2048, 1024], P('ep', None, 'tp'), may hold values from -0.125 to 0.125
- expert_up: bfloat16 [8, 2048, 1024], P('ep', None, 'tp'), may hold values from -0.125 to 0.125
- expert_down: bfloat16 [8, 1024, 2048], P('ep', 'tp')
- dense_switch: bfloat16 [2048], replicated, may hold values from -0.125 to 0.125
- dense_gate: bfloat16 [2048, 2048], P('ep', 'tp'), may hold values from -0.125 to 0.125
- dense_up: bfloat16 [2048, 2048], P('ep', 'tp'), may hold values from -0.125 to 0.125
- dense_down: bfloat16 [2048, 2048], P('ep', 'tp')
- out_gain: bfloat16 [2048], P('tp'), may hold values from 0.099609375 to 1.8984375
Outputs:
- layer_out: bfloat16 [256, 2048], P('ep', 'tp')
- new_state: float32 [256, 8, 64, 128], P('ep', 'tp')
- new_conv: bfloat16 [256, 3, 3, 512], P('ep', None, None, 'tp')
Inputs may be any that keep to these rules, and one draw needn't show every extreme that they name: `route_experts`: each row names 4 different experts, all from one group of 4 consecutive expert numbers. Within each aligned block of 32 rows (the rows of one index of ep) no expert is named more than 32 times, and one expert, the same in every block, is named exactly 32 times in every block.
All inputs are finite; a program needn't handle non-finite values.
Results may differ from a plain program's by a relative error of at most 0.019.
Values may be sent and summed in bfloat16 or wider, within the bound.
A program may use at most 64 MiB of HBM per device.

v0:
```python
import jax
import jax.numpy as jnp
from jax import lax
from jax.sharding import PartitionSpec as P

norm_eps = 1e-06


def scaled_rows(values, gain):
    values = values.astype(jnp.float32)
    mean_square = jnp.mean(values * values, axis=-1, keepdims=True)
    return values * lax.rsqrt(mean_square + norm_eps) * gain.astype(jnp.float32)


def softmax_plain(logits):
    weights = jnp.exp(logits)
    return weights / jnp.sum(weights, axis=-1, keepdims=True)


def on_device(
    resid,
    mix_gain,
    proj_x,
    proj_z,
    proj_b,
    proj_c,
    proj_step,
    step_bias,
    decay_rate,
    conv_taps,
    conv_state,
    scan_state,
    inner_gain,
    proj_out,
    post_gain,
    ffn_gain,
    group_router,
    expert_router,
    route_experts,
    expert_gate,
    expert_up,
    expert_down,
    dense_switch,
    dense_gate,
    dense_up,
    dense_down,
    out_gain,
):
    tp_index = lax.axis_index("tp")
    seqs = resid.shape[0]
    width = resid.shape[1]
    quarter = width // lax.axis_size("tp")
    heads_here = scan_state.shape[1]
    head_dim = scan_state.shape[2]
    state_dim = scan_state.shape[3]
    channels = conv_state.shape[3]
    repeat = heads_here // (channels // state_dim)
    normed = scaled_rows(resid, mix_gain).astype(jnp.bfloat16)
    fresh = jnp.stack(
        [
            jnp.dot(normed, proj_x, preferred_element_type=jnp.float32),
            jnp.dot(normed, proj_b, preferred_element_type=jnp.float32),
            jnp.dot(normed, proj_c, preferred_element_type=jnp.float32),
        ],
        axis=1,
    ).astype(jnp.bfloat16)
    gate_z = jnp.dot(normed, proj_z, preferred_element_type=jnp.float32)
    step_all = jnp.dot(normed, proj_step, preferred_element_type=jnp.float32)
    step_raw = lax.dynamic_slice_in_dim(step_all, tp_index * heads_here, heads_here, 1)
    history = jnp.concatenate([conv_state, fresh[:, :, None, :]], axis=2)
    activated = jax.nn.silu(
        jnp.sum(history.astype(jnp.float32) * conv_taps.astype(jnp.float32)[None], axis=2)
    )
    xs_heads = activated[:, 0].reshape(seqs, heads_here, head_dim)
    b_heads = jnp.repeat(activated[:, 1].reshape(seqs, -1, state_dim), repeat, axis=1)
    c_heads = jnp.repeat(activated[:, 2].reshape(seqs, -1, state_dim), repeat, axis=1)
    step = jax.nn.softplus(step_raw + step_bias)
    keep = jnp.exp(-decay_rate * step)
    driven = step[:, :, None] * xs_heads
    new_state = keep[:, :, None, None] * scan_state + driven[:, :, :, None] * b_heads[:, :, None, :]
    read = jnp.sum(new_state * c_heads[:, :, None, :], axis=3).reshape(seqs, channels)
    gated = (read * jax.nn.silu(gate_z) * inner_gain.astype(jnp.float32)).astype(jnp.bfloat16)
    mixed = lax.psum(
        jnp.dot(gated, proj_out, preferred_element_type=jnp.float32).astype(jnp.bfloat16), "tp"
    ).astype(jnp.float32)
    stream = (resid.astype(jnp.float32) + scaled_rows(mixed, post_gain)).astype(jnp.bfloat16)
    feed = scaled_rows(stream, ffn_gain).astype(jnp.bfloat16)
    feed_quarter = lax.dynamic_slice_in_dim(feed, tp_index * quarter, quarter, 1)
    expert_count = expert_router.shape[1]
    group_size = expert_count // group_router.shape[1]
    pick_count = route_experts.shape[1]
    group_prob = softmax_plain(jnp.dot(feed, group_router, preferred_element_type=jnp.float32))
    expert_logits = jnp.dot(feed, expert_router, preferred_element_type=jnp.float32)
    matches = route_experts[:, :, None] == jnp.arange(expert_count, dtype=jnp.int32)[None, None, :]
    pick_logits = jnp.sum(jnp.where(matches, expert_logits[:, None, :], 0.0), axis=2)
    chosen_group = route_experts[:, 0] // group_size
    group_ids = jnp.arange(group_router.shape[1], dtype=jnp.int32)
    group_weight = jnp.sum(
        jnp.where(chosen_group[:, None] == group_ids[None, :], group_prob, 0.0), axis=1
    )
    pick_weight = softmax_plain(pick_logits) * group_weight[:, None]
    capacity = 2 * seqs * pick_count // expert_count
    flat_picks = route_experts.reshape(-1)
    one_hot = (flat_picks[:, None] == jnp.arange(expert_count, dtype=jnp.int32)[None, :]).astype(
        jnp.int32
    )
    slot = jnp.sum((jnp.cumsum(one_hot, axis=0) - one_hot) * one_hot, axis=1)
    target = flat_picks * capacity + slot
    repeated = jnp.repeat(feed, pick_count, axis=0)
    outgoing = jnp.zeros((expert_count * capacity, width), jnp.bfloat16).at[target].set(repeated)
    outgoing = outgoing.reshape(expert_count, capacity, width)
    arrived = lax.all_to_all(outgoing, "ep", split_axis=0, concat_axis=0, tiled=True)
    sources = arrived.shape[0]
    items = arrived.shape[1]
    rows = arrived.reshape(sources * items, width)
    gate_value = jnp.dot(rows, expert_gate[0], preferred_element_type=jnp.float32)
    up_value = jnp.dot(rows, expert_up[0], preferred_element_type=jnp.float32)
    hidden = (jax.nn.silu(gate_value) * up_value).astype(jnp.bfloat16)
    result = jnp.dot(hidden, expert_down[0], preferred_element_type=jnp.float32).reshape(
        sources, items, width
    )
    summed = lax.psum_scatter(result.astype(jnp.bfloat16), "tp", scatter_dimension=2, tiled=True)
    returned = lax.all_to_all(summed, "ep", split_axis=0, concat_axis=0, tiled=True)
    fetched = returned.reshape(expert_count * capacity, quarter)[target].reshape(
        seqs, pick_count, quarter
    )
    routed = jnp.sum(fetched.astype(jnp.float32) * pick_weight[:, :, None], axis=1)
    gate_piece = jnp.einsum(
        "sd,cd->sc",
        feed_quarter,
        lax.all_gather(dense_gate, "ep", axis=0, tiled=True),
        preferred_element_type=jnp.float32,
    )
    up_piece = jnp.einsum(
        "sd,cd->sc",
        feed_quarter,
        lax.all_gather(dense_up, "ep", axis=0, tiled=True),
        preferred_element_type=jnp.float32,
    )
    gate_sum = gate_piece
    up_sum = up_piece
    gate_sum, up_sum = (
        lax.psum(gate_sum.astype(jnp.bfloat16), "tp").astype(jnp.float32),
        lax.psum(up_sum.astype(jnp.bfloat16), "tp").astype(jnp.float32),
    )
    dense_hidden = (jax.nn.silu(gate_sum) * up_sum).astype(jnp.bfloat16)
    dense_out = jnp.dot(
        dense_hidden,
        lax.all_gather(dense_down, "ep", axis=0, tiled=True),
        preferred_element_type=jnp.float32,
    )
    switch = jax.nn.sigmoid(jnp.dot(feed, dense_switch, preferred_element_type=jnp.float32))
    combined = routed + switch[:, None] * dense_out
    total_square = lax.psum(jnp.sum(combined * combined, axis=1), "tp")
    scale = lax.rsqrt(total_square / width + norm_eps)
    stream_part = lax.dynamic_slice_in_dim(stream, tp_index * quarter, quarter, 1).astype(
        jnp.float32
    )
    layer_out = (stream_part + combined * scale[:, None] * out_gain.astype(jnp.float32)).astype(
        jnp.bfloat16
    )
    new_conv = history[:, :, 1:, :]
    return (layer_out, new_state, new_conv)


def solution(mesh):
    placed = (
        P("ep", None),
        P(),
        P(None, "tp"),
        P(None, "tp"),
        P(None, "tp"),
        P(None, "tp"),
        P(),
        P("tp"),
        P("tp"),
        P(None, None, "tp"),
        P("ep", None, None, "tp"),
        P("ep", "tp", None, None),
        P("tp"),
        P("tp", None),
        P(),
        P(),
        P(),
        P(),
        P("ep", None),
        P("ep", None, "tp"),
        P("ep", None, "tp"),
        P("ep", "tp", None),
        P(),
        P("ep", "tp"),
        P("ep", "tp"),
        P("ep", "tp"),
        P("tp"),
    )
    return jax.shard_map(
        on_device,
        mesh=mesh,
        in_specs=placed,
        out_specs=(P("ep", "tp"), P("ep", "tp", None, None), P("ep", None, None, "tp")),
        check_vma=False,
    )
```

profile of v0, /device:TPU:0, one launch (start us, length us, event | category | flops | bytes accessed | tf_op | source)
XLA Modules:
  0.0 219.6 jit_solution(17043526989973223200)
XLA Ops:
  9.0 1.1 fusion.24
  10.1 1.4 fusion.2
  11.4 1.4 fusion.3
  12.8 1.4 fusion.4
  14.2 0.9 multiply_reduce_fusion.2
  15.3 1.0 fusion.48
  16.7 2.1 multiply_reduce_fusion
  18.9 2.3 %convolution_convert_fusion.3 = bf16[32,2048]{1,0:T(8,128)(2,1)} fusion(bf16[128,2048]{1,0:T(8,128)(2,1)} %param.40, f32[32,128]{1,0:T(8,128)S(1)} %reshape.185, f32[128]{0:T(128)S(1)} %convert_element_type.95, bf16[2048,128]{1,0:T(8,128)(2,1)} %param.30, bf16[32,2048]{1,0:T(8,128)(2,1)S(1)} %copy-done.1, f32[2048]{0:T(1024)S(1)} %convert_element_type.91, ...), kind=kOutput, calls=%fused_computation.5 | convolution fusion | flops 33910784 | bytes 1335936 | tf_op jit(solution)/shard_map/dot_general | solution.py:84
  22.8 33.1 %all-reduce.4.cloned.1.call-done = bf16[32,2048]{1,0:T(8,128)(2,1)} async-done(((bf16[32,2048]{1,0:T(8,128)(2,1)}), bf16[32,2048]{1,0:T(8,128)(2,1)}) %all-reduce.4.cloned.1.call-update) | async-done | bytes 131088 | tf_op jit(solution)/shard_map/psum | solution.py:83
  55.9 1.0 fusion.15
  57.0 1.2 fusion.17
  58.5 0.9 reshape.203
  59.4 2.2 %scatter_custom_fusion = bf16[256,2048]{1,0:T(8,128)(2,1)S(1)} fusion(s32[128]{0:T(128)S(1)} %fusion.39, bf16[128,2048]{1,0:T(8,128)(2,1)} %reshape.203, bf16[]{:T(256)} %constant.57.clone.1), kind=kCustom, calls=%fused_computation.28 | custom fusion | bytes 1049088 | tf_op jit(solution)/shard_map/scatter | solution.py:110
  61.7 36.1 %all_to_all.10 = bf16[8,32,2048]{2,1,0:T(8,128)(2,1)S(1)} all-to-all(bf16[8,32,2048]{2,1,0:T(8,128)(2,1)S(1)} %bitcast.63), channel_id=1, replica_groups=mesh['ep'=8,'tp'=4] {'ep'}, dimensions={0} | all-to-all | bytes 2097152 | tf_op jit(solution)/shard_map/all_to_all | solution.py:112
  98.7 1.4 convolution_convert_fusion
  102.6 3.1 %convolution_convert_fusion.1 = bf16[32,2048]{1,0:T(8,128)(2,1)} fusion(bf16[2048,512]{1,0:T(8,128)(2,1)} %all-gather.6.cloned.1.call-done, bf16[32,2048]{1,0:T(8,128)(2,1)S(1)} %fusion.19, s32[]{:T(128)S(6)} %select_n.38), kind=kOutput, calls=%fused_computation.3 | convolution fusion | flops 67174400 | bytes 2260996 | tf_op jit(solution)/shard_map/sd,cd->sc/dot_general | solution.py:134
  105.7 17.5 %reduce-scatter.2.cloned.1.call-done = bf16[8,32,512]{2,1,0:T(8,128)(2,1)} async-done(((bf16[8,32,2048]{2,1,0:T(8,128)(2,1)}), bf16[8,32,512]{2,1,0:T(8,128)(2,1)}) %reduce-scatter.2.cloned.1.call-update) | async-done | bytes 262160 | tf_op jit(solution)/shard_map/reduce_scatter | solution.py:122
  123.2 5.5 %all-to-all-start.1 = ((bf16[8,32,512]{2,1,0:T(8,128)(2,1)}), bf16[8,32,512]{2,1,0:T(8,128)(2,1)S(1)}, u32[]{:S(2)}, u32[]{:S(2)}) async-start(bf16[8,32,512]{2,1,0:T(8,128)(2,1)} %reduce-scatter.2.cloned.1.call-done), calls=%async_computation.2 | async-start | bytes 524288 | tf_op jit(solution)/shard_map/all_to_all | solution.py:123
  128.8 24.4 %all-gather.4.cloned.1.call-done = bf16[2048,512]{1,0:T(8,128)(2,1)} async-done(((bf16[256,512]{1,0:T(8,128)(2,1)}), bf16[2048,512]{1,0:T(8,128)(2,1)}) %all-gather.4.cloned.1.call-update) | async-done | bytes 2097168 | tf_op jit(solution)/shard_map/all_gather | solution.py:131
  153.2 3.0 %convolution_convert_fusion.2 = bf16[32,2048]{1,0:T(8,128)(2,1)} fusion(bf16[2048,512]{1,0:T(8,128)(2,1)} %all-gather.4.cloned.1.call-done, bf16[32,2048]{1,0:T(8,128)(2,1)S(1)} %fusion.19, s32[]{:T(128)S(6)} %select_n.38), kind=kOutput, calls=%fused_computation.4 | convolution fusion | flops 67174400 | bytes 2260996 | tf_op jit(solution)/shard_map/sd,cd->sc/dot_general | solution.py:128
  156.3 0.8 gather_fusion
  157.5 46.1 %all-gather.8.cloned.1.call-done = bf16[2048,512]{1,0:T(8,128)(2,1)} async-done(((bf16[256,512]{1,0:T(8,128)(2,1)}), bf16[2048,512]{1,0:T(8,128)(2,1)}) %all-gather.8.cloned.1.call-update) | async-done | bytes 2097168 | tf_op jit(solution)/shard_map/all_gather | solution.py:149
  203.6 2.3 %multiply_reduce_fusion.3 = (f32[32]{0:T(128)S(1)}, f32[32,512]{1,0:T(8,128)S(1)}) fusion(f32[32,512]{1,0:T(8,128)S(1)} %multiply_reduce_fusion.1, bf16[2048,512]{1,0:T(8,128)(2,1)} %all-gather.8.cloned.1.call-done, bf16[32,2048]{1,0:T(8,128)(2,1)} %get-tuple-element.3, bf16[32,2048]{1,0:T(8,128)(2,1)} %get-tuple-element.4, f32[32]{0:T(128)S(1)} %fusion.8), kind=kOutput, calls=%fused_computation.58 | convolution fusion | flops 67698656 | bytes 2490624 | tf_op jit(solution)/shard_map/dot_general | solution.py:147
  205.9 5.7 %psum.31 = f32[32]{0:T(128)S(1)} all-reduce(f32[32]{0:T(128)S(1)} %get-tuple-element.18), channel_id=1, replica_groups=mesh['ep'=8,'tp'=4] {'tp'}, use_global_device_ids=true, to_apply=%region_18.19 | all-reduce | flops 32 | bytes 256 | tf_op jit(solution)/shard_map/psum | solution.py:154
  (94 shorter events, 7.8 us)
Async XLA Ops:
  8.0 90.7 %copy-start = (bf16[1,256,2048]{2,1,0:T(8,128)(2,1)S(1)}, bf16[1,256,2048]{2,1,0:T(8,128)(2,1)}, u32[]{:S(2)}) copy-start(bf16[1,256,2048]{2,1,0:T(8,128)(2,1)} %param.48) | copy-start | bytes 3145732
  8.0 7.3 %copy-start.1 = (bf16[32,2048]{1,0:T(8,128)(2,1)S(1)}, bf16[32,2048]{1,0:T(8,128)(2,1)}, u32[]{:S(2)}) copy-start(bf16[32,2048]{1,0:T(8,128)(2,1)} %param.27) | copy-start | bytes 393220
  8.0 6.2 %copy-start.9 = (bf16[3,4,128]{2,1,0:T(4,128)(2,1)S(1)}, bf16[3,4,128]{2,1,0:T(4,128)(2,1)}, u32[]{:S(2)}) copy-start(bf16[3,4,128]{2,1,0:T(4,128)(2,1)} %param.36) | copy-start | bytes 9220
  8.0 8.2 %copy-start.14 = (f32[2]{0:T(128)S(1)}, f32[2]{0:T(128)}, u32[]{:S(2)}) copy-start(f32[2]{0:T(128)} %param.35) | copy-start | bytes 28
  8.0 8.2 %copy-start.11 = (f32[2]{0:T(128)S(1)}, f32[2]{0:T(128)}, u32[]{:S(2)}) copy-start(f32[2]{0:T(128)} %param.34) | copy-start | bytes 28
  8.1 8.6 %copy-start.2 = (f32[32,2,64,128]{3,2,1,0:T(8,128)S(1)}, f32[32,2,64,128]{3,2,1,0:T(8,128)}, u32[]{:S(2)}) copy-start(f32[32,2,64,128]{3,2,1,0:T(8,128)} %param.38) | copy-start | bytes 6291460
  8.1 47.9 %all-reduce.4.cloned.1.call-start = ((), (), s32[]{:S(2)}) async-start(), calls=%async_computation.3 | async-start | bytes 262144 | tf_op jit(solution)/shard_map/psum | solution.py:83
  16.7 2.2 %copy-start.15 = (bf16[128]{0:T(256)(128)(2,1)S(1)}, bf16[128]{0:T(256)(128)(2,1)}, u32[]{:S(2)}) copy-start(bf16[128]{0:T(256)(128)(2,1)} %param.39) | copy-start | bytes 772
  16.7 5.2 %copy-start.5 = (s32[32,4]{0,1:T(4,128)S(1)}, s32[32,4]{0,1:T(4,128)}, u32[]{:S(2)}) copy-start(s32[32,4]{0,1:T(4,128)} %param.45) | copy-start | bytes 1540
  16.7 5.3 %copy-start.6 = (bf16[2048]{0:T(1024)(128)(2,1)S(1)}, bf16[2048]{0:T(1024)(128)(2,1)}, u32[]{:S(2)}) copy-start(bf16[2048]{0:T(1024)(128)(2,1)} %param.41) | copy-start | bytes 12292
  16.7 5.3 %copy-start.7 = (bf16[2048]{0:T(1024)(128)(2,1)S(1)}, bf16[2048]{0:T(1024)(128)(2,1)}, u32[]{:S(2)}) copy-start(bf16[2048]{0:T(1024)(128)(2,1)} %param.42) | copy-start | bytes 12292
  21.3 81.3 %all-gather.6.cloned.1.call-start = ((), (), s32[]{:S(2)}) async-start(), calls=%async_computation.6 | async-start | bytes 2359296 | tf_op jit(solution)/shard_map/all_gather | solution.py:137
  21.9 101.4 %reduce-scatter.2.cloned.1.call-start = ((), (), s32[]{:S(2)}) async-start(), calls=%async_computation.4 | async-start | bytes 1310720 | tf_op jit(solution)/shard_map/reduce_scatter | solution.py:122
  58.5 39.2 %copy-start.3 = (bf16[1,2048,256]{2,1,0:T(8,128)(2,1)S(1)}, bf16[1,2048,256]{2,1,0:T(8,128)(2,1)}, u32[]{:S(2)}) copy-start(bf16[1,2048,256]{2,1,0:T(8,128)(2,1)} %param.46) | copy-start | bytes 3145732
  61.6 36.5 %copy-start.12 = (bf16[1,2048,256]{2,1,0:T(8,128)(2,1)S(1)}, bf16[1,2048,256]{2,1,0:T(8,128)(2,1)}, u32[]{:S(2)}) copy-start(bf16[1,2048,256]{2,1,0:T(8,128)(2,1)} %param.47) | copy-start | bytes 3145732
  98.6 2.7 %copy-start.8 = (bf16[2048]{0:T(1024)(128)(2,1)S(1)}, bf16[2048]{0:T(1024)(128)(2,1)}, u32[]{:S(2)}) copy-start(bf16[2048]{0:T(1024)(128)(2,1)} %param.49) | copy-start | bytes 12292
  98.6 2.7 %copy-start.10 = (bf16[512]{0:T(512)(128)(2,1)S(1)}, bf16[512]{0:T(512)(128)(2,1)}, u32[]{:S(2)}) copy-start(bf16[512]{0:T(512)(128)(2,1)} %param.53) | copy-start | bytes 3076
  98.7 3.4 %copy-start.4 = (bf16[2048,8]{0,1:T(8,128)(2,1)S(1)}, bf16[2048,8]{0,1:T(8,128)(2,1)}, u32[]{:S(2)}) copy-start(bf16[2048,8]{0,1:T(8,128)(2,1)} %param.44) | copy-start | bytes 98308
  98.7 3.6 %copy-start.13 = (bf16[2048,2]{0,1:T(2,128)(2,1)S(1)}, bf16[2048,2]{0,1:T(2,128)(2,1)}, u32[]{:S(2)}) copy-start(bf16[2048,2]{0,1:T(2,128)(2,1)} %param.43) | copy-start | bytes 24580
  100.2 53.1 %all-gather.4.cloned.1.call-start = ((), (), s32[]{:S(2)}) async-start(), calls=%async_computation.5 | async-start | bytes 2359296 | tf_op jit(solution)/shard_map/all_gather | solution.py:131
  100.7 102.8 %all-gather.8.cloned.1.call-start = ((), (), s32[]{:S(2)}) async-start(), calls=%async_computation.7 | async-start | bytes 2359296 | tf_op jit(solution)/shard_map/all_gather | solution.py:149
  123.2 33.1 %all-to-all-start.1 = ((bf16[8,32,512]{2,1,0:T(8,128)(2,1)}), bf16[8,32,512]{2,1,0:T(8,128)(2,1)S(1)}, u32[]{:S(2)}, u32[]{:S(2)}) async-start(bf16[8,32,512]{2,1,0:T(8,128)(2,1)} %reduce-scatter.2.cloned.1.call-done), calls=%async_computation.2 | async-start | bytes 524288 | tf_op jit(solution)/shard_map/all_to_all | solution.py:123
  128.8 74.8 %all-reduce.6.cloned.1.call-start = ((), (), s32[]{:S(2)}) async-start(), calls=%async_computation.8 | async-start | bytes 524288 | tf_op jit(solution)/shard_map/psum | solution.py:144
Sparse Core Ops, SparseCore 0:
  21.4 34.4 all-reduce.3
  100.3 22.9 reduce-scatter.1
  156.3 31.6 all-reduce.5
Sparse Core Ops, SparseCore 1:
  23.9 59.7 all-gather.5
  102.8 50.4 all-gather.3
  155.2 48.3 all-gather.7
where the time goes:
time: 220 us
  waiting for transfers between devices  123 us (56%)
  blocking collectives  41.7 us (19%)
  matrix products  18.6 us (8%)
  between operations  15.9 us (7%)
  other arithmetic  8.99 us (4%)
  local copies, waits for them, and re-layouts  5.86 us (3%)
  starting transfers between devices  5.78 us (3%)
    all_gather x1, waiting for transfers between devices, on_device(): lax.all_gather(dense_down, 'ep', axis=0, tiled=True)  46.1 us
    all_to_all x1, blocking collectives, on_device(): lax.all_to_all(outgoing, 'ep', split_axis=0, concat_axis=0, tiled=True)  36.1 us
    psum x1, waiting for transfers between devices, on_device(): lax.psum(jnp.dot(gated, proj_out, preferred_element_type=jnp.float32).ast...  33.1 us
    all_gather x1, waiting for transfers between devices, on_device(): lax.all_gather(dense_gate, 'ep', axis=0, tiled=True)  24.4 us
    reduce_scatter x1, waiting for transfers between devices, on_device(): lax.psum_scatter(result.astype(jnp.bfloat16), 'tp', scatter_dimension=2,...  17.5 us
    psum x1, blocking collectives, on_device(): total_square = lax.psum(jnp.sum(combined * combined, axis=1), 'tp')  5.67 us
    all_to_all x1, starting transfers between devices, on_device(): lax.all_to_all(summed, 'ep', split_axis=0, concat_axis=0, tiled=True)  5.53 us
  transfers between devices with their start and end apart: 7, of which 4 were waited for; matrix products, arithmetic and copies ran while one was open for 8% of the time, Pallas kernels for 0%

commit v1 on v0

--- a/solution.py
+++ b/solution.py
@@ -1,9 +1,18 @@
+import functools
 import jax
 import jax.numpy as jnp
 from jax import lax
 from jax.sharding import PartitionSpec as P
 
 norm_eps = 1e-06
+
+
+def clusters_set(message, row_axis):
+    y2 = jnp.sum(lax.all_gather(message, row_axis), axis=0)
+    return y2
+
+
+fit_the_trees = functools.partial(clusters_set, row_axis="tp")
 
 
 def scaled_rows(values, gain):
@@ -80,8 +89,8 @@
     new_state = keep[:, :, None, None] * scan_state + driven[:, :, :, None] * b_heads[:, :, None, :]
     read = jnp.sum(new_state * c_heads[:, :, None, :], axis=3).reshape(seqs, channels)
     gated = (read * jax.nn.silu(gate_z) * inner_gain.astype(jnp.float32)).astype(jnp.bfloat16)
-    mixed = lax.psum(
-        jnp.dot(gated, proj_out, preferred_element_type=jnp.float32).astype(jnp.bfloat16), "tp"
+    mixed = fit_the_trees(
+        jnp.dot(gated, proj_out, preferred_element_type=jnp.float32).astype(jnp.bfloat16)
     ).astype(jnp.float32)
     stream = (resid.astype(jnp.float32) + scaled_rows(mixed, post_gain)).astype(jnp.bfloat16)
     feed = scaled_rows(stream, ffn_gain).astype(jnp.bfloat16)

time: 220 us -> 240 us (1.091)
  waiting for transfers between devices: 123 us -> 139 us
  blocking collectives: 41.7 us -> 46.3 us
    psum x1 -> x0, waiting for transfers between devices: 33.1 us -> none  [on_device(): lax.psum(jnp.dot(gated, proj_out, preferred_element_type=jnp.float32).ast...]
    all_gather x1, waiting for transfers between devices: 0.01 us -> 24.4 us  [on_device(): lax.all_gather(dense_up, 'ep', axis=0, tiled=True)]
    all_gather x1, waiting for transfers between devices: 24.4 us -> 47.4 us  [on_device(): lax.all_gather(dense_gate, 'ep', axis=0, tiled=True)]
    all_gather x0 -> x1, blocking collectives: none -> 8.65 us  [clusters_set(): y2 = jnp.sum(lax.all_gather(message, row_axis), axis=0)]
    all_to_all x1, blocking collectives: 36.1 us -> 32 us  [on_device(): lax.all_to_all(outgoing, 'ep', split_axis=0, concat_axis=0, tiled=True)]
    reduce_scatter x1, waiting for transfers between devices: 17.5 us -> 21.2 us  [on_device(): lax.psum_scatter(result.astype(jnp.bfloat16), 'tp', scatter_dimension=2,...]
  transfers between devices with their start and end apart: 7 -> 6, of which waited for: 4 -> 4; matrix products, arithmetic and copies ran while one was open for 8% -> 3% of each run, Pallas kernels for 0% -> 0%
where the time goes in v1:
time: 240 us
  waiting for transfers between devices  139 us (58%)
  blocking collectives  46.3 us (19%)
  matrix products  17.7 us (7%)
  between operations  16.1 us (7%)
  other arithmetic  7.76 us (3%)
  local copies, waits for them, and re-layouts  6.69 us (3%)
  starting transfers between devices  5.72 us (2%)
    all_gather x1, waiting for transfers between devices, on_device(): lax.all_gather(dense_gate, 'ep', axis=0, tiled=True)  47.4 us
    all_gather x1, waiting for transfers between devices, on_device(): lax.all_gather(dense_down, 'ep', axis=0, tiled=True)  44.7 us
    all_to_all x1, blocking collectives, on_device(): lax.all_to_all(outgoing, 'ep', split_axis=0, concat_axis=0, tiled=True)  32 us
    all_gather x1, waiting for transfers between devices, on_device(): lax.all_gather(dense_up, 'ep', axis=0, tiled=True)  24.4 us
    reduce_scatter x1, waiting for transfers between devices, on_device(): lax.psum_scatter(result.astype(jnp.bfloat16), 'tp', scatter_dimension=2,...  21.2 us
    all_gather x1, blocking collectives, clusters_set(): y2 = jnp.sum(lax.all_gather(message, row_axis), axis=0)  8.65 us
    psum x1, blocking collectives, on_device(): total_square = lax.psum(jnp.sum(combined * combined, axis=1), 'tp')  5.67 us
    all_to_all x1, starting transfers between devices, on_device(): lax.all_to_all(summed, 'ep', split_axis=0, concat_axis=0, tiled=True)  5.51 us
  transfers between devices with their start and end apart: 6, of which 4 were waited for; matrix products, arithmetic and copies ran while one was open for 3% of the time, Pallas kernels for 0%

profile of v1, /device:TPU:0, one launch (start us, length us, event | category | flops | bytes accessed | tf_op | source)
XLA Modules:
  0.0 239.6 jit_solution(16604459808767391345)
XLA Ops:
  8.1 0.9 copy.45
  10.4 1.0 fusion.24
  11.5 1.4 fusion.2
  12.9 1.4 fusion.3
  14.3 1.4 fusion.4
  15.7 0.9 multiply_reduce_fusion.2
  16.7 1.0 fusion.48
  18.1 2.1 multiply_reduce_fusion
  20.3 1.7 convolution_convert_fusion.3
  22.0 8.7 %all-gather = bf16[128,2048]{1,0:T(8,128)(2,1)S(1)} all-gather(bf16[32,2048]{1,0:T(8,128)(2,1)S(1)} %convolution_convert_fusion.3), channel_id=2, replica_groups=mesh['ep'=8,'tp'=4] {'tp'}, dimensions={0}, use_global_device_ids=true | all-gather | bytes 655360 | tf_op jit(solution)/shard_map/all_gather | solution.py:11
  31.5 0.9 reshape.203
  33.2 2.2 scatter_custom_fusion
  35.4 32.0 %all_to_all.10 = bf16[8,32,2048]{2,1,0:T(8,128)(2,1)S(1)} all-to-all(bf16[8,32,2048]{2,1,0:T(8,128)(2,1)S(1)} %bitcast.64), channel_id=1, replica_groups=mesh['ep'=8,'tp'=4] {'ep'}, dimensions={0} | all-to-all | bytes 2097152 | tf_op jit(solution)/shard_map/all_to_all | solution.py:121
  68.4 1.4 convolution_convert_fusion
  72.2 21.2 %reduce-scatter.2.cloned.1.call-done = bf16[8,32,512]{2,1,0:T(8,128)(2,1)} async-done(((bf16[8,32,2048]{2,1,0:T(8,128)(2,1)}), bf16[8,32,512]{2,1,0:T(8,128)(2,1)}) %reduce-scatter.2.cloned.1.call-update) | async-done | bytes 262160 | tf_op jit(solution)/shard_map/reduce_scatter | solution.py:131
  93.5 5.5 %all-to-all-start.1 = ((bf16[8,32,512]{2,1,0:T(8,128)(2,1)}), bf16[8,32,512]{2,1,0:T(8,128)(2,1)S(1)}, u32[]{:S(2)}, u32[]{:S(2)}) async-start(bf16[8,32,512]{2,1,0:T(8,128)(2,1)} %reduce-scatter.2.cloned.1.call-done), calls=%async_computation.2 | async-start | bytes 524288 | tf_op jit(solution)/shard_map/all_to_all | solution.py:132
  99.0 24.4 %all-gather.7.cloned.1.call-done = bf16[2048,512]{1,0:T(8,128)(2,1)} async-done(((bf16[256,512]{1,0:T(8,128)(2,1)}), bf16[2048,512]{1,0:T(8,128)(2,1)}) %all-gather.7.cloned.1.call-update) | async-done | bytes 2097168 | tf_op jit(solution)/shard_map/all_gather | solution.py:146
  123.5 3.0 %convolution_convert_fusion.1 = bf16[32,2048]{1,0:T(8,128)(2,1)} fusion(bf16[2048,512]{1,0:T(8,128)(2,1)} %all-gather.7.cloned.1.call-done, bf16[32,2048]{1,0:T(8,128)(2,1)S(1)} %fusion.19, s32[]{:T(128)S(6)} %select_n.38), kind=kOutput, calls=%fused_computation.3 | convolution fusion | flops 67174400 | bytes 2260996 | tf_op jit(solution)/shard_map/sd,cd->sc/dot_general | solution.py:143
  126.4 47.4 %all-gather.5.cloned.1.call-done = bf16[2048,512]{1,0:T(8,128)(2,1)} async-done(((bf16[256,512]{1,0:T(8,128)(2,1)}), bf16[2048,512]{1,0:T(8,128)(2,1)}) %all-gather.5.cloned.1.call-update) | async-done | bytes 2097168 | tf_op jit(solution)/shard_map/all_gather | solution.py:140
  173.8 3.0 %convolution_convert_fusion.2 = bf16[32,2048]{1,0:T(8,128)(2,1)} fusion(bf16[2048,512]{1,0:T(8,128)(2,1)} %all-gather.5.cloned.1.call-done, bf16[32,2048]{1,0:T(8,128)(2,1)S(1)} %fusion.19, s32[]{:T(128)S(6)} %select_n.38), kind=kOutput, calls=%fused_computation.4 | convolution fusion | flops 67174400 | bytes 2260996 | tf_op jit(solution)/shard_map/sd,cd->sc/dot_general | solution.py:137
  177.5 0.8 gather_fusion
  178.7 44.7 %all-gather.9.cloned.1.call-done = bf16[2048,512]{1,0:T(8,128)(2,1)} async-done(((bf16[256,512]{1,0:T(8,128)(2,1)}), bf16[2048,512]{1,0:T(8,128)(2,1)}) %all-gather.9.cloned.1.call-update) | async-done | bytes 2097168 | tf_op jit(solution)/shard_map/all_gather | solution.py:158
  223.4 2.3 multiply_reduce_fusion.3
  225.7 5.7 %psum.23 = f32[32]{0:T(128)S(1)} all-reduce(f32[32]{0:T(128)S(1)} %get-tuple-element.18), channel_id=1, replica_groups=mesh['ep'=8,'tp'=4] {'tp'}, use_global_device_ids=true, to_apply=%region_18.19 | all-reduce | flops 32 | bytes 256 | tf_op jit(solution)/shard_map/psum | solution.py:163
  (93 shorter events, 8.6 us)
Async XLA Ops:
  8.0 60.4 %copy-start = (bf16[1,256,2048]{2,1,0:T(8,128)(2,1)S(1)}, bf16[1,256,2048]{2,1,0:T(8,128)(2,1)}, u32[]{:S(2)}) copy-start(bf16[1,256,2048]{2,1,0:T(8,128)(2,1)} %param.48) | copy-start | bytes 3145732
  8.0 8.7 %copy-start.1 = (bf16[32,2048]{1,0:T(8,128)(2,1)S(1)}, bf16[32,2048]{1,0:T(8,128)(2,1)}, u32[]{:S(2)}) copy-start(bf16[32,2048]{1,0:T(8,128)(2,1)} %param.27) | copy-start | bytes 393220
  8.0 7.6 %copy-start.9 = (bf16[3,4,128]{2,1,0:T(4,128)(2,1)S(1)}, bf16[3,4,128]{2,1,0:T(4,128)(2,1)}, u32[]{:S(2)}) copy-start(bf16[3,4,128]{2,1,0:T(4,128)(2,1)} %param.36) | copy-start | bytes 9220
  8.0 9.7 %copy-start.14 = (f32[2]{0:T(128)S(1)}, f32[2]{0:T(128)}, u32[]{:S(2)}) copy-start(f32[2]{0:T(128)} %param.35) | copy-start | bytes 28
  8.0 9.7 %copy-start.11 = (f32[2]{0:T(128)S(1)}, f32[2]{0:T(128)}, u32[]{:S(2)}) copy-start(f32[2]{0:T(128)} %param.34) | copy-start | bytes 28
  8.1 10.1 %copy-start.2 = (f32[32,2,64,128]{3,2,1,0:T(8,128)S(1)}, f32[32,2,64,128]{3,2,1,0:T(8,128)}, u32[]{:S(2)}) copy-start(f32[32,2,64,128]{3,2,1,0:T(8,128)} %param.38) | copy-start | bytes 6291460
  8.1 85.4 %reduce-scatter.2.cloned.1.call-start = ((), (), s32[]{:S(2)}) async-start(), calls=%async_computation.3 | async-start | bytes 1310720 | tf_op jit(solution)/shard_map/reduce_scatter | solution.py:131
  18.1 2.2 copy-start.15
  20.2 10.7 %copy-start.6 = (bf16[2048]{0:T(1024)(128)(2,1)S(1)}, bf16[2048]{0:T(1024)(128)(2,1)}, u32[]{:S(2)}) copy-start(bf16[2048]{0:T(1024)(128)(2,1)} %param.41) | copy-start | bytes 12292
  20.2 10.9 %copy-start.7 = (bf16[2048]{0:T(1024)(128)(2,1)S(1)}, bf16[2048]{0:T(1024)(128)(2,1)}, u32[]{:S(2)}) copy-start(bf16[2048]{0:T(1024)(128)(2,1)} %param.42) | copy-start | bytes 12292
  31.5 35.9 %copy-start.3 = (bf16[1,2048,256]{2,1,0:T(8,128)(2,1)S(1)}, bf16[1,2048,256]{2,1,0:T(8,128)(2,1)}, u32[]{:S(2)}) copy-start(bf16[1,2048,256]{2,1,0:T(8,128)(2,1)} %param.46) | copy-start | bytes 3145732
  35.4 32.5 %copy-start.12 = (bf16[1,2048,256]{2,1,0:T(8,128)(2,1)S(1)}, bf16[1,2048,256]{2,1,0:T(8,128)(2,1)}, u32[]{:S(2)}) copy-start(bf16[1,2048,256]{2,1,0:T(8,128)(2,1)} %param.47) | copy-start | bytes 3145732
  68.3 3.3 %copy-start.8 = (bf16[2048]{0:T(1024)(128)(2,1)S(1)}, bf16[2048]{0:T(1024)(128)(2,1)}, u32[]{:S(2)}) copy-start(bf16[2048]{0:T(1024)(128)(2,1)} %param.49) | copy-start | bytes 12292
  68.4 3.3 %copy-start.4 = (bf16[2048,8]{0,1:T(8,128)(2,1)S(1)}, bf16[2048,8]{0,1:T(8,128)(2,1)}, u32[]{:S(2)}) copy-start(bf16[2048,8]{0,1:T(8,128)(2,1)} %param.44) | copy-start | bytes 98308
  68.4 3.4 %copy-start.5 = (s32[32,4]{0,1:T(4,128)S(1)}, s32[32,4]{0,1:T(4,128)}, u32[]{:S(2)}) copy-start(s32[32,4]{0,1:T(4,128)} %param.45) | copy-start | bytes 1540
  68.4 3.5 %copy-start.13 = (bf16[2048,2]{0,1:T(2,128)(2,1)S(1)}, bf16[2048,2]{0,1:T(2,128)(2,1)}, u32[]{:S(2)}) copy-start(bf16[2048,2]{0,1:T(2,128)(2,1)} %param.43) | copy-start | bytes 24580
  69.9 53.6 %all-gather.7.cloned.1.call-start = ((), (), s32[]{:S(2)}) async-start(), calls=%async_computation.5 | async-start | bytes 2359296 | tf_op jit(solution)/shard_map/all_gather | solution.py:146
  70.5 103.4 %all-gather.5.cloned.1.call-start = ((), (), s32[]{:S(2)}) async-start(), calls=%async_computation.4 | async-start | bytes 2359296 | tf_op jit(solution)/shard_map/all_gather | solution.py:140
  71.0 152.4 %all-gather.9.cloned.1.call-start = ((), (), s32[]{:S(2)}) async-start(), calls=%async_computation.6 | async-start | bytes 2359296 | tf_op jit(solution)/shard_map/all_gather | solution.py:158
  93.5 84.1 %all-to-all-start.1 = ((bf16[8,32,512]{2,1,0:T(8,128)(2,1)}), bf16[8,32,512]{2,1,0:T(8,128)(2,1)S(1)}, u32[]{:S(2)}, u32[]{:S(2)}) async-start(bf16[8,32,512]{2,1,0:T(8,128)(2,1)} %reduce-scatter.2.cloned.1.call-done), calls=%async_computation.2 | async-start | bytes 524288 | tf_op jit(solution)/shard_map/all_to_all | solution.py:132
  99.0 77.9 %copy-start.10 = (bf16[512]{0:T(512)(128)(2,1)S(1)}, bf16[512]{0:T(512)(128)(2,1)}, u32[]{:S(2)}) copy-start(bf16[512]{0:T(512)(128)(2,1)} %param.53) | copy-start | bytes 3076
  99.0 124.4 %all-reduce.3.cloned.1.call-start = ((), (), s32[]{:S(2)}) async-start(), calls=%async_computation.7 | async-start | bytes 524288 | tf_op jit(solution)/shard_map/psum | solution.py:153
Sparse Core Ops, SparseCore 0:
  70.0 23.4 reduce-scatter.1
  176.9 30.9 all-reduce.2
Sparse Core Ops, SparseCore 1:
  72.5 50.9 all-gather.6
  125.5 48.3 all-gather.4
  175.8 47.5 all-gather.8
